TPU v7x, 32 devices: a whole 2x2x4 slice. The times are simulated.
32 devices in a mesh: sp: 4 (over z), fs: 4 (over y, x), tp: 2 (over core).
Axes of the slice: x: 2, y: 2, z: 4, core: 2. Of those that a mesh axis runs over, the one named last changes fastest.
Arguments:
- inputs: bfloat16 [4, 512, 2048], P('fs', 'sp'), may hold values from -9 to 9
- norm_gain: float32 [2048], replicated, may hold values from 0.1 to 1.9
- hg_query_w: bfloat16 [2048, 1024], P(('sp', 'fs'), 'tp'), may hold values from -0.125 to 0.125
- hg_fwd_w: bfloat16 [2048, 1024], P(('sp', 'fs'), 'tp'), may hold values from -0.125 to 0.125
- hg_bwd_w: bfloat16 [2048, 1024], P(('sp', 'fs'), 'tp'), may hold values from -0.125 to 0.125
- hg_value_w: bfloat16 [2048, 1024], P(('sp', 'fs'), 'tp'), may hold values from -0.125 to 0.125
- floor_gap: float32 [2, 1024], P(None, 'tp'), may hold values from 0 to 0.1
- hg_norm_gain: float32 [64], replicated, may hold values from 0.1 to 1.9
- df_query_w: bfloat16 [2048, 512], P(('sp', 'fs'), 'tp'), may hold values from -0.176776695 to 0.176776695
- df_key_w: bfloat16 [2048, 512], P(('sp', 'fs'), 'tp'), may hold values from -4.4194174 to 4.4194174
- df_value_w: bfloat16 [2048, 512], P(('sp', 'fs'), 'tp'), may hold values from -0.125 to 0.125
- diff_lambda: float32 [8], P('tp'), may hold values from 0.3 to 0.8
- df_norm_gain: float32 [64], replicated, may hold values from 0.1 to 1.9
- out_hg_w: bfloat16 [1024, 2048], P('tp'), may hold values from -0.15625 to 0.15625
- out_df_w: bfloat16 [512, 2048], P('tp'), may hold values from -0.15625 to 0.15625
- post_gain: float32 [2048], replicated, may hold values from 0.1 to 1.9
Outputs:
- mixed: bfloat16 [4, 512, 2048], P('fs', ('sp', 'tp'))
All inputs are finite; a program needn't handle non-finite values.
Results may differ from a plain program's by a relative error of at most 0.017.
Values may be sent and summed in bfloat16 or wider, within the bound.
A program may use at most 64 MiB of HBM per device.

v0:
```python
import jax
import jax.numpy as jnp
from jax import lax
from jax.sharding import PartitionSpec as P

HEAD = 64
DQK = 32
BLOCK = 64
DFV = 64


epsilon = 1e-06
df_factor = 0.8
highest_precision = lax.Precision.HIGHEST


def rms_scale(values):
    return lax.rsqrt(jnp.mean(values * values, axis=-1, keepdims=True) + epsilon)


def span_scan(queries, taken, values, kept_log):
    head_count, length, key_dim = queries.shape
    blocks = length // BLOCK

    def to_blocks(tensor):
        return tensor.reshape(head_count, blocks, BLOCK, tensor.shape[-1]).transpose(1, 0, 2, 3)

    lower_mask = jnp.tril(jnp.ones((BLOCK, BLOCK), dtype=bool))[:, :, None]

    def advance(state_stack, pieces):
        query_block, key_block, value_block, g_blk = pieces
        cumulative_log = jnp.cumsum(g_blk, axis=1)
        across_blocks = jnp.einsum(
            "bqy,byo->bqo",
            query_block * jnp.exp(cumulative_log),
            state_stack,
            precision=highest_precision,
        )
        spread = cumulative_log[:, :, None, :] - cumulative_log[:, None, :, :]
        decays = jnp.where(lower_mask, jnp.exp(jnp.where(lower_mask, spread, 0.0)), 0.0)
        scores = jnp.einsum(
            "hik,hijk->hij",
            query_block,
            decays * key_block[:, None, :, :],
            precision=highest_precision,
        )
        inside = jnp.einsum("hij,hjv->hiv", scores, value_block, precision=highest_precision)
        final_log_decay = cumulative_log[:, -1:, :]
        carried = jnp.exp(final_log_decay[:, 0, :])[..., None] * state_stack
        fresh_portion = jnp.einsum(
            "moc,moa->mca",
            key_block * jnp.exp(final_log_decay - cumulative_log),
            value_block,
            precision=highest_precision,
        )
        return (carried + fresh_portion, across_blocks + inside)

    start_state = jnp.zeros((head_count, key_dim, values.shape[-1]), jnp.float32)
    final_state, outputs = lax.scan(
        advance,
        start_state,
        (to_blocks(queries), to_blocks(taken), to_blocks(values), to_blocks(kept_log)),
    )
    return (
        outputs.transpose(1, 0, 2, 3).reshape(head_count, length, values.shape[-1]),
        final_state,
    )


def key_width(row_count):
    for candidate in range(min(row_count, 1024), 0, -1):
        if row_count % candidate == 0:
            return candidate
    return 1


def shards(
    inputs,
    norm_gain,
    hg_query_w,
    hg_fwd_w,
    hg_bwd_w,
    hg_value_w,
    floor_gap,
    hg_norm_gain,
    df_query_w,
    df_key_w,
    df_value_w,
    diff_lambda,
    df_norm_gain,
    out_hg_w,
    out_df_w,
    post_gain,
):
    tok_rows = inputs[0]
    length = tok_rows.shape[0]
    rows_float = tok_rows.astype(jnp.float32)
    normed = (rows_float * rms_scale(rows_float) * norm_gain).astype(jnp.bfloat16)
    pieces = (
        lax.all_gather(hg_query_w, ("sp", "fs"), axis=0, tiled=True),
        lax.all_gather(hg_fwd_w, ("sp", "fs"), axis=0, tiled=True),
        lax.all_gather(hg_bwd_w, ("sp", "fs"), axis=0, tiled=True),
        lax.all_gather(hg_value_w, ("sp", "fs"), axis=0, tiled=True),
        lax.all_gather(df_query_w, ("sp", "fs"), axis=0, tiled=True),
        lax.all_gather(df_key_w, ("sp", "fs"), axis=0, tiled=True),
        lax.all_gather(df_value_w, ("sp", "fs"), axis=0, tiled=True),
    )
    summed = tuple((jnp.dot(normed, piece, preferred_element_type=jnp.float32) for piece in pieces))
    hg_query, hg_fwd, hg_bwd, hg_value, df_query, df_key, df_value = [
        member.astype(jnp.bfloat16) for member in summed
    ]
    heads_hg = hg_query.shape[1] // HEAD

    def split_heads(tensor):
        return tensor.astype(jnp.float32).reshape(length, heads_hg, HEAD).transpose(1, 0, 2)

    queries = jax.nn.silu(split_heads(hg_query))
    values = split_heads(hg_value)

    def summarize(raw_gate, gap_row, flipped):
        taken = gap_row.reshape(heads_hg, 1, HEAD) * jax.nn.sigmoid(-split_heads(raw_gate))
        series = (queries, taken, values, jnp.log1p(-taken))
        if flipped:
            series = tuple((jnp.flip(tensor, axis=1) for tensor in series))
        local_out, final_state = span_scan(*series)
        cumulative_log = jnp.cumsum(series[3], axis=1)
        return (
            local_out,
            final_state,
            jnp.exp(cumulative_log[:, -1, :]),
            series[0] * jnp.exp(cumulative_log),
        )

    forward_output, fwd_state, fwd_decay, forward_reader = summarize(hg_fwd, floor_gap[0], False)
    backward_output, bwd_state, bwd_decay, backward_reader = summarize(hg_bwd, floor_gap[1], True)
    all_decay, all_state = (
        lax.all_gather(
            jnp.stack([fwd_decay, bwd_decay])[None].astype(jnp.bfloat16), "sp", axis=0, tiled=True
        ).astype(jnp.float32),
        lax.all_gather(
            jnp.stack([fwd_state, bwd_state])[None].astype(jnp.bfloat16), "sp", axis=0, tiled=True
        ).astype(jnp.float32),
    )
    position = lax.axis_index("sp")
    members = all_decay.shape[0]

    def forward_step(member, running):
        joined = all_decay[member, 0][..., None] * running + all_state[member, 0]
        return jnp.where(member < position, joined, running)

    def backward_step(offset, running):
        member = members - 1 - offset
        joined = all_decay[member, 1][..., None] * running + all_state[member, 1]
        return jnp.where(member > position, joined, running)

    forward_carry = lax.fori_loop(0, members, forward_step, jnp.zeros_like(fwd_state))
    backward_carry = lax.fori_loop(0, members, backward_step, jnp.zeros_like(bwd_state))
    forward_sum = forward_output + jnp.einsum(
        "bqy,byo->bqo", forward_reader, forward_carry, precision=highest_precision
    )
    bwd_total = jnp.flip(
        backward_output
        + jnp.einsum("bqy,byo->bqo", backward_reader, backward_carry, precision=highest_precision),
        axis=1,
    )
    recurrent = forward_sum + bwd_total
    hg_out = (
        (recurrent * rms_scale(recurrent) * hg_norm_gain)
        .transpose(1, 0, 2)
        .reshape(length, heads_hg * HEAD)
        .astype(jnp.bfloat16)
    )
    heads_df = df_value.shape[1] // DFV
    df_queries = df_query.reshape(length, heads_df, 2, DQK)
    score_scale = DQK ** (-0.5)
    start_carry = (
        jnp.full((heads_df, 2, length), -1e30, jnp.float32),
        jnp.zeros((heads_df, 2, length), jnp.float32),
        jnp.zeros((heads_df, 2, length, DFV), jnp.float32),
    )
    carry = start_carry
    key_rows = lax.all_gather(df_key, "sp", axis=0, tiled=True)
    value_rows = lax.all_gather(df_value, "sp", axis=0, tiled=True)
    row_count = key_rows.shape[0]
    block_rows = key_width(row_count)
    key_blocks = key_rows.reshape(row_count // block_rows, block_rows, heads_df, 2, DQK)
    value_blocks = value_rows.reshape(row_count // block_rows, block_rows, heads_df, DFV)

    def key_step(running, block_pair):
        tops, totals, accums = running
        key_blk, value_blk = block_pair
        scores = (
            jnp.einsum("qhmd,khmd->hmqk", df_queries, key_blk, preferred_element_type=jnp.float32)
            * score_scale
        )
        new_tops = jnp.maximum(tops, jnp.max(scores, axis=-1))
        factor = jnp.exp(tops - new_tops)
        weights_blk = jnp.exp(scores - new_tops[..., None])
        totals = totals * factor + jnp.sum(weights_blk, axis=-1)
        accums = accums * factor[..., None] + jnp.einsum(
            "hmqk,khd->hmqd",
            weights_blk.astype(jnp.bfloat16),
            value_blk,
            preferred_element_type=jnp.float32,
        )
        return ((new_tops, totals, accums), None)

    carry, unused = lax.scan(key_step, carry, (key_blocks, value_blocks))
    tops, totals, accums = carry
    maps = accums / totals[..., None]
    weighted = maps[:, 0] - diff_lambda[:, None, None] * maps[:, 1]
    df_out = (
        (weighted * rms_scale(weighted) * df_norm_gain * df_factor)
        .transpose(1, 0, 2)
        .reshape(length, heads_df * DFV)
        .astype(jnp.bfloat16)
    )
    mixture = lax.psum_scatter(
        (
            jnp.dot(hg_out, out_hg_w, preferred_element_type=jnp.float32)
            + jnp.dot(df_out, out_df_w, preferred_element_type=jnp.float32)
        ).astype(jnp.bfloat16),
        "tp",
        scatter_dimension=0,
        tiled=True,
    ).astype(jnp.float32)
    return (mixture * rms_scale(mixture) * post_gain).astype(jnp.bfloat16)[None]


def solution(mesh):
    in_specs = (
        P("fs", "sp", None),
        P(),
        P(("sp", "fs"), "tp"),
        P(("sp", "fs"), "tp"),
        P(("sp", "fs"), "tp"),
        P(("sp", "fs"), "tp"),
        P(None, "tp"),
        P(),
        P(("sp", "fs"), "tp"),
        P(("sp", "fs"), "tp"),
        P(("sp", "fs"), "tp"),
        P("tp"),
        P(),
        P("tp", None),
        P("tp", None),
        P(),
    )
    out_specs = P("fs", ("sp", "tp"), None)
    return jax.shard_map(shards, mesh=mesh, in_specs=in_specs, out_specs=out_specs, check_vma=False)
```

profile of v0, /device:TPU:0, one launch (start us, length us, event | category | flops | bytes accessed | tf_op | source)
XLA Modules:
  0.0 678.6 jit_solution(10265758264301679093)
XLA Ops:
  11.3 1.2 fusion.77
  13.5 54.4 %all-gather.18.cloned.1.call-done = bf16[2048,256]{1,0:T(8,128)(2,1)} async-done(((bf16[128,256]{1,0:T(8,128)(2,1)}), bf16[2048,256]{1,0:T(8,128)(2,1)}) %all-gather.18.cloned.1.call-update) | async-done | bytes 1048592 | tf_op jit(solution)/shard_map/all_gather | solution.py:105
  67.9 1.8 convolution_convert_fusion.5
  69.7 55.0 %all-gather.16.cloned.1.call-done = bf16[2048,256]{1,0:T(8,128)(2,1)} async-done(((bf16[128,256]{1,0:T(8,128)(2,1)}), bf16[2048,256]{1,0:T(8,128)(2,1)}) %all-gather.16.cloned.1.call-update) | async-done | bytes 1048592 | tf_op jit(solution)/shard_map/all_gather | solution.py:104
  124.7 2.2 convolution_convert_fusion.6
  126.9 54.5 %all-gather.20.cloned.1.call-done = bf16[2048,256]{1,0:T(8,128)(2,1)} async-done(((bf16[128,256]{1,0:T(8,128)(2,1)}), bf16[2048,256]{1,0:T(8,128)(2,1)}) %all-gather.20.cloned.1.call-update) | async-done | bytes 1048592 | tf_op jit(solution)/shard_map/all_gather | solution.py:106
  181.4 1.6 convolution_convert_fusion.4
  183.0 15.1 %all_gather.41 = bf16[512,256]{1,0:T(8,128)(2,1)} all-gather(bf16[128,256]{1,0:T(8,128)(2,1)S(1)} %convolution_convert_fusion.5), channel_id=1, replica_groups=mesh['sp'=4,'fs'=4,'tp'=2] {'sp'}, dimensions={0}, use_global_device_ids=true | all-gather | bytes 327680 | tf_op jit(solution)/shard_map/all_gather | solution.py:182
  200.2 15.1 %all_gather.43 = bf16[512,256]{1,0:T(8,128)(2,1)} all-gather(bf16[128,256]{1,0:T(8,128)(2,1)S(1)} %convolution_convert_fusion.4), channel_id=1, replica_groups=mesh['sp'=4,'fs'=4,'tp'=2] {'sp'}, dimensions={0}, use_global_device_ids=true | all-gather | bytes 327680 | tf_op jit(solution)/shard_map/all_gather | solution.py:183
  215.2 1.8 copy.101
  219.4 1.4 fusion.109
  220.8 22.8 %all-gather.10.cloned.1.call-done = bf16[2048,512]{1,0:T(8,128)(2,1)} async-done(((bf16[128,512]{1,0:T(8,128)(2,1)}), bf16[2048,512]{1,0:T(8,128)(2,1)}) %all-gather.10.cloned.1.call-update) | async-done | bytes 2097168 | tf_op jit(solution)/shard_map/all_gather | solution.py:103
  243.7 2.8 fusion.72
  249.5 56.0 %all-gather.8.cloned.1.call-done = bf16[2048,512]{1,0:T(8,128)(2,1)} async-done(((bf16[128,512]{1,0:T(8,128)(2,1)}), bf16[2048,512]{1,0:T(8,128)(2,1)}) %all-gather.8.cloned.1.call-update) | async-done | bytes 2097168 | tf_op jit(solution)/shard_map/all_gather | solution.py:101
  305.5 2.1 fusion.76
  308.9 58.4 %all-gather.12.cloned.1.call-done = bf16[2048,512]{1,0:T(8,128)(2,1)} async-done(((bf16[128,512]{1,0:T(8,128)(2,1)}), bf16[2048,512]{1,0:T(8,128)(2,1)}) %all-gather.12.cloned.1.call-update) | async-done | bytes 2097168 | tf_op jit(solution)/shard_map/all_gather | solution.py:100
  367.3 2.2 fusion.71
  370.4 1.9 copy.85
  372.4 23.2 %fusion.107 = f32[8,128,64]{2,0,1:T(8,128)S(1)} fusion(f32[8,128,64]{2,0,1:T(8,128)S(1)} %copy.110), kind=kOutput, calls=%fused_computation.164 | output fusion | flops 8323072 | bytes 524288 | tf_op jit(solution)/shard_map/jit(cumsum)/reduce_window_sum | solution.py:126
  396.4 2.0 exponential_multiply_fusion.3
  399.3 30.0 %all-gather.14.cloned.1.call-done = bf16[2048,512]{1,0:T(8,128)(2,1)} async-done(((bf16[128,512]{1,0:T(8,128)(2,1)}), bf16[2048,512]{1,0:T(8,128)(2,1)}) %all-gather.14.cloned.1.call-update) | async-done | bytes 2097168 | tf_op jit(solution)/shard_map/all_gather | solution.py:102
  429.3 3.0 fusion.70
  436.5 1.2 fusion.108
  439.2 1.8 rev.17
  441.0 2.0 copy.113
  444.9 77.5 %while.67 = (s32[]{:T(128)}, f32[8,64,64]{2,1,0:T(8,128)S(1)}, f32[2,8,64,64]{3,2,1,0:T(8,128)}, f32[2,8,64,64]{3,1,2,0:T(8,128)}, f32[2,8,64,64]{3,1,2,0:T(8,12...) while((s32[]{:T(128)}, f32[8,64,64]{2,1,0:T(8,128)S(1)}, ...), condition=%wide.region_8.9_spmd.clone.clone, body=%wide.region_6.8_spmd.clone.clone.sunk | while | flops 111382528 | bytes 6050988 | solution.py:59
  446.0 1.9 exponential_multiply_fusion.8
  448.1 30.0 %fusion.196 = f32[8,64,1,64]{3,2,1,0:T(1,128)} fusion(f32[8,64,64]{2,1,0:T(8,128)S(1)} %copy.153, f32[8,64,64]{2,1,0:T(8,128)S(1)} %copy.154, pred[64,64]{1,0:T(8,128)(4,1)S(1)} %fusion.195, f32[8,64,64,1]{2,0,1,3:T(8,128)S(1)} %dynamic-slice_bitcast_fusion.15), kind=kOutput, calls=%fused_computation.45.clone.1 | convolution fusion | flops 33554432 | bytes 528384 | tf_op jit(solution)/shard_map/while/body/eval_jaxpr/hik,hijk->hij/dot_general | solution.py:41
  478.1 1.4 fusion.194
  479.5 1.3 constant_dynamic-slice_fusion.5
  480.8 2.2 fusion.197
  484.8 1.9 exponential_multiply_fusion.8
  486.9 30.0 %fusion.196 = f32[8,64,1,64]{3,2,1,0:T(1,128)} fusion(f32[8,64,64]{2,1,0:T(8,128)S(1)} %copy.153, f32[8,64,64]{2,1,0:T(8,128)S(1)} %copy.154, pred[64,64]{1,0:T(8,128)(4,1)S(1)} %fusion.195, f32[8,64,64,1]{2,0,1,3:T(8,128)S(1)} %dynamic-slice_bitcast_fusion.15), kind=kOutput, calls=%fused_computation.45.clone.1 | convolution fusion | flops 33554432 | bytes 528384 | tf_op jit(solution)/shard_map/while/body/eval_jaxpr/hik,hijk->hij/dot_general | solution.py:41
  516.9 1.4 fusion.194
  518.3 1.3 constant_dynamic-slice_fusion.5
  519.6 2.2 fusion.197
  522.4 2.0 copy.111
  525.3 77.2 %while.66 = (s32[]{:T(128)}, f32[8,64,64]{2,1,0:T(8,128)S(1)}, f32[2,8,64,64]{3,2,1,0:T(8,128)}, f32[2,8,64,64]{3,1,2,0:T(8,128)}, f32[2,8,64,64]{3,1,2,0:T(8,12...) while((s32[]{:T(128)}, f32[8,64,64]{2,1,0:T(8,128)S(1)}, ...), condition=%wide.region_3.4_spmd.clone.clone, body=%wide.region_1.3_spmd.clone.clone.sunk | while | flops 111382528 | bytes 5002384 | solution.py:59
  526.3 1.8 exponential_multiply_fusion.7
  528.3 30.0 %fusion.181 = f32[8,64,1,64]{3,2,1,0:T(1,128)} fusion(f32[8,64,64]{2,1,0:T(8,128)S(1)} %copy.148, f32[8,64,64]{2,1,0:T(8,128)S(1)} %copy.149, pred[64,64]{1,0:T(8,128)(4,1)S(1)} %fusion.180, f32[8,64,64,1]{2,0,1,3:T(8,128)S(1)} %dynamic-slice_bitcast_fusion.14), kind=kOutput, calls=%fused_computation.8.clone.1 | convolution fusion | flops 33554432 | bytes 528384 | tf_op jit(solution)/shard_map/while/body/eval_jaxpr/hik,hijk->hij/dot_general | solution.py:41
  558.3 1.4 fusion.179
  559.7 1.3 constant_dynamic-slice_fusion.4
  561.0 2.3 fusion.182
  565.0 1.8 exponential_multiply_fusion.7
  566.9 30.0 %fusion.181 = f32[8,64,1,64]{3,2,1,0:T(1,128)} fusion(f32[8,64,64]{2,1,0:T(8,128)S(1)} %copy.148, f32[8,64,64]{2,1,0:T(8,128)S(1)} %copy.149, pred[64,64]{1,0:T(8,128)(4,1)S(1)} %fusion.180, f32[8,64,64,1]{2,0,1,3:T(8,128)S(1)} %dynamic-slice_bitcast_fusion.14), kind=kOutput, calls=%fused_computation.8.clone.1 | convolution fusion | flops 33554432 | bytes 528384 | tf_op jit(solution)/shard_map/while/body/eval_jaxpr/hik,hijk->hij/dot_general | solution.py:41
  596.9 1.4 fusion.179
  598.3 1.3 constant_dynamic-slice_fusion.4
  599.7 2.2 fusion.182
  602.7 21.4 %all_gather.38 = bf16[4,2,8,64,64]{4,3,2,1,0:T(8,128)(2,1)S(1)} all-gather(bf16[1,2,8,64,64]{4,3,2,1,0:T(8,128)(2,1)S(1)} %pad_maximum_fusion), channel_id=1, replica_groups=mesh['sp'=4,'fs'=4,'tp'=2] {'sp'}, dimensions={0}, use_global_device_ids=true | all-gather | bytes 655360 | tf_op jit(solution)/shard_map/all_gather | solution.py:140
  624.1 1.6 convert_element_type.103
  625.7 13.2 %all_gather.37 = bf16[4,2,8,64]{3,2,1,0:T(8,128)(2,1)S(1)} all-gather(bf16[1,2,8,64]{3,2,1,0:T(8,128)(2,1)S(1)} %pad_maximum_fusion.1), channel_id=1, replica_groups=mesh['sp'=4,'fs'=4,'tp'=2] {'sp'}, dimensions={0}, use_global_device_ids=true | all-gather | bytes 10240 | tf_op jit(solution)/shard_map/all_gather | solution.py:137
  638.9 5.0 while.64
  644.0 4.9 while.65
  644.0 1.2 fusion.167
  645.3 1.2 fusion.167
  648.9 2.0 copy.96
  650.9 1.3 reshape.257
  652.3 1.9 convolution_add_fusion.5
  655.3 2.1 copy.87
  657.3 1.3 reshape.252
  658.7 1.2 multiply_reduce_fusion.1
  660.0 2.5 fusion.62
  662.6 6.3 reduce-scatter.2.cloned.1.call-done
  670.0 1.8 fusion.91
  (154 shorter events, 42.1 us)
Async XLA Ops:
  6.5 653.5 %copy-start = (bf16[512,2048]{1,0:T(8,128)(2,1)S(1)}, bf16[512,2048]{1,0:T(8,128)(2,1)}, u32[]{:S(2)}) copy-start(bf16[512,2048]{1,0:T(8,128)(2,1)} %param.37) | copy-start | bytes 6291460
  6.5 118.1 %copy-start.7 = (bf16[1,128,2048]{2,1,0:T(8,128)(2,1)S(1)}, bf16[1,128,2048]{2,1,0:T(8,128)(2,1)}, u32[]{:S(2)}) copy-start(bf16[1,128,2048]{2,1,0:T(8,128)(2,1)} %param.24) | copy-start | bytes 1572868
  6.5 118.1 %copy-start.14 = (f32[2048]{0:T(1024)S(1)}, f32[2048]{0:T(1024)}, u32[]{:S(2)}) copy-start(f32[2048]{0:T(1024)} %param.25) | copy-start | bytes 24580
  6.5 61.4 %all-gather.18.cloned.1.call-start = ((), (), s32[]{:S(2)}) async-start(), calls=%async_computation.6 | async-start | bytes 1114112 | tf_op jit(solution)/shard_map/all_gather | solution.py:105
  7.3 117.4 %all-gather.16.cloned.1.call-start = ((), (), s32[]{:S(2)}) async-start(), calls=%async_computation.5 | async-start | bytes 1114112 | tf_op jit(solution)/shard_map/all_gather | solution.py:104
  8.0 173.4 %all-gather.20.cloned.1.call-start = ((), (), s32[]{:S(2)}) async-start(), calls=%async_computation.7 | async-start | bytes 1114112 | tf_op jit(solution)/shard_map/all_gather | solution.py:106
  8.7 234.9 %all-gather.10.cloned.1.call-start = ((), (), s32[]{:S(2)}) async-start(), calls=%async_computation.2 | async-start | bytes 2228224 | tf_op jit(solution)/shard_map/all_gather | solution.py:103
  9.3 296.2 %all-gather.8.cloned.1.call-start = ((), (), s32[]{:S(2)}) async-start(), calls=%async_computation.1 | async-start | bytes 2228224 | tf_op jit(solution)/shard_map/all_gather | solution.py:101
  9.9 357.4 %all-gather.12.cloned.1.call-start = ((), (), s32[]{:S(2)}) async-start(), calls=%async_computation.3 | async-start | bytes 2228224 | tf_op jit(solution)/shard_map/all_gather | solution.py:100
  10.5 418.8 %all-gather.14.cloned.1.call-start = ((), (), s32[]{:S(2)}) async-start(), calls=%async_computation.4 | async-start | bytes 2228224 | tf_op jit(solution)/shard_map/all_gather | solution.py:102
  11.2 657.6 %reduce-scatter.2.cloned.1.call-start = ((), (), s32[]{:S(2)}) async-start(), calls=%async_computation.8 | async-start | bytes 786432 | tf_op jit(solution)/shard_map/reduce_scatter | solution.py:218
  12.6 170.4 %copy-start.17 = (f32[128]{0:T(128)}, f32[128]{0:T(128)S(1)}, u32[]{:S(2)}) copy-start(f32[128]{0:T(128)S(1)} %add_rsqrt_fusion.3) | copy-start | bytes 1540
  217.0 1.2 copy-start.13
  218.2 0.7 copy-start.16
  218.2 0.8 copy-start.19
  218.2 1.2 copy-start.12
  218.9 24.8 %copy-start.18 = (f32[128]{0:T(128)S(1)}, f32[128]{0:T(128)}, u32[]{:S(2)}) copy-start(f32[128]{0:T(128)} %copy-done.17) | copy-start | bytes 1540
  308.9 63.5 %copy-start.4 = (f32[8,128,64]{2,0,1:T(8,128)}, f32[8,128,64]{2,0,1:T(8,128)S(1)}, u32[]{:S(2)}) copy-start(f32[8,128,64]{2,0,1:T(8,128)S(1)} %copy.110) | copy-start | bytes 786436
  395.6 0.8 copy-start.8
  436.5 6.5 copy-start.11
  444.9 3.1 copy-start.3
  478.1 5.0 copy-start.1
  483.7 3.1 copy-start.3
  516.9 4.9 copy-start.1
  558.3 5.0 copy-start.2
  596.9 5.0 copy-start.2
  602.7 36.2 %copy-start.6 = (f32[8,64,64]{2,1,0:T(8,128)S(1)}, f32[8,64,64]{2,1,0:T(8,128)}, u32[]{:S(2)}) copy-start(f32[8,64,64]{2,1,0:T(8,128)} %custom-call) | copy-start | bytes 393220
  638.9 5.1 copy-start.5
  644.0 8.3 %copy-start.9 = (f32[8,128,64]{2,0,1:T(8,128)S(1)}, f32[8,128,64]{2,0,1:T(8,128)}, u32[]{:S(2)}) copy-start(f32[8,128,64]{2,0,1:T(8,128)} %exponential_multiply_fusion.2) | copy-start | bytes 786436
  654.1 4.5 copy-start.10
  654.1 5.8 copy-start.20
  660.0 10.0 %copy-start.15 = (f32[2048]{0:T(1024)S(1)}, f32[2048]{0:T(1024)}, u32[]{:S(2)}) copy-start(f32[2048]{0:T(1024)} %param.39) | copy-start | bytes 24580
Sparse Core Ops, SparseCore 0:
  10.1 57.7 all-gather.17
  70.7 53.9 all-gather.15
  127.4 53.9 all-gather.19
  184.0 59.6 all-gather.9
  246.3 59.1 all-gather.7
  308.1 59.1 all-gather.11
  370.1 59.1 all-gather.13
  662.7 6.1 reduce-scatter.1
where the time goes:
time: 681 us; the launch traced here: 679 us
  waiting for transfers between devices  342 us (50%)
  matrix products  161 us (24%)
  blocking collectives  64.8 us (10%)
  other arithmetic  57.5 us (8%)
  local copies, waits for them, and re-layouts  38.5 us (6%)
  between operations  13.9 us (2%)
    dot_general x4, matrix products, advance(): jnp.einsum('hik,hijk->hij', query_block, decays * key_block[:, None, :, :...  120 us
    all_gather x1, waiting for transfers between devices, shards(): lax.all_gather(hg_query_w, ('sp', 'fs'), axis=0, tiled=True)  58.4 us
    all_gather x1, waiting for transfers between devices, shards(): lax.all_gather(hg_fwd_w, ('sp', 'fs'), axis=0, tiled=True)  56 us
    all_gather x1, waiting for transfers between devices, shards(): lax.all_gather(df_query_w, ('sp', 'fs'), axis=0, tiled=True)  55 us
    all_gather x1, waiting for transfers between devices, shards(): lax.all_gather(df_value_w, ('sp', 'fs'), axis=0, tiled=True)  54.5 us
    all_gather x1, waiting for transfers between devices, shards(): lax.all_gather(df_key_w, ('sp', 'fs'), axis=0, tiled=True)  54.4 us
    all_gather x1, waiting for transfers between devices, shards(): lax.all_gather(hg_bwd_w, ('sp', 'fs'), axis=0, tiled=True)  30 us
    another operation x2, other arithmetic, summarize(): cumulative_log = jnp.cumsum(series[3], axis=1)  24.5 us
  transfers between devices with their start and end apart: 8, of which 8 were waited for; matrix products, arithmetic and copies ran while one was open for 8% of the time, Pallas kernels for 0%

commit v1 on v0

--- a/solution.py
+++ b/solution.py
@@ -1,6 +1,11 @@
+import functools
+import math
+
 import jax
 import jax.numpy as jnp
 from jax import lax
+from jax.experimental import pallas as pl
+from jax.experimental.pallas import tpu as pltpu
 from jax.sharding import PartitionSpec as P
 
 HEAD = 64
@@ -74,7 +79,7 @@
     return 1
 
 
-def shards(
+def spread_shards(
     inputs,
     norm_gain,
     hg_query_w,
@@ -227,7 +232,293 @@
     return (mixture * rms_scale(mixture) * post_gain).astype(jnp.bfloat16)[None]
 
 
+MESH = pl.DeviceIdType.MESH
+VMEM_SPEC = pl.BlockSpec(memory_space=pltpu.VMEM)
+ANY_SPEC = pl.BlockSpec(memory_space=pl.ANY)
+STEEPEST = -math.log1p(-0.1)
+
+
+def greet(peers):
+    barrier = pltpu.get_barrier_semaphore()
+    for peer in peers:
+        pl.semaphore_signal(barrier, inc=1, device_id=peer, device_id_type=MESH)
+    pl.semaphore_wait(barrier, len(peers))
+
+
+def gather_kernel(n_sp, n_fs, wp_ref, x_ref, wg_ref, xg_ref, own_sem, s1, r1, sx, rx, s2, r2):
+    sp, fs = lax.axis_index("sp"), lax.axis_index("fs")
+    sp_peers = [lax.rem(sp + d, n_sp) for d in range(1, n_sp)]
+    fs_peers = [lax.rem(fs + e, n_fs) for e in range(1, n_fs)]
+    greet([{"sp": p} for p in sp_peers] + [{"fs": p} for p in fs_peers])
+
+    def remote(src, dst, send, recv, peer):
+        return pltpu.make_async_remote_copy(
+            src_ref=src, dst_ref=dst, send_sem=send, recv_sem=recv, device_id=peer, device_id_type=MESH
+        )
+
+    started = []
+    along = []
+    for d, peer in enumerate(sp_peers):
+        copy = remote(wp_ref.at[peer], wg_ref.at[sp, fs], s1.at[d], r1.at[d], {"sp": peer})
+        copy.start()
+        along.append(copy)
+    for e, peer in enumerate(fs_peers):
+        copy = remote(wp_ref.at[sp], wg_ref.at[sp, fs], s2.at[0, e], r2.at[0, e], {"fs": peer})
+        copy.start()
+        started.append(copy)
+    for d, peer in enumerate(sp_peers):
+        copy = remote(x_ref, xg_ref.at[sp], sx.at[d], rx.at[d], {"sp": peer})
+        copy.start()
+        started.append(copy)
+    own_w = pltpu.make_async_copy(wp_ref.at[sp], wg_ref.at[sp, fs], own_sem.at[0])
+    own_x = pltpu.make_async_copy(x_ref, xg_ref.at[sp], own_sem.at[1])
+    own_w.start()
+    own_x.start()
+    for d in range(n_sp - 1):
+        along[d].wait_recv()
+        source = lax.rem(sp + n_sp - d - 1, n_sp)
+        for e, peer in enumerate(fs_peers):
+            piece = wg_ref.at[source, fs]
+            copy = remote(piece, piece, s2.at[d + 1, e], r2.at[d + 1, e], {"fs": peer})
+            copy.start()
+            started.append(copy)
+    own_w.wait()
+    own_x.wait()
+    for copy in along:
+        copy.wait_send()
+    for copy in started:
+        copy.wait()
+
+
+def mixer_kernel(
+    hr, ha, x_ref, w_ref, gain_ref, gap_ref, hgain_ref, lam_ref, dgain_ref, o_ref, proj_ref
+):
+    length = x_ref.shape[0]
+    rows = min(length, 128)
+    for start in range(0, length, rows):
+        x = x_ref[start : start + rows, :].astype(jnp.float32)
+        scale = lax.rsqrt(jnp.mean(x * x, axis=-1, keepdims=True) + epsilon)
+        normed = (x * scale * gain_ref[...]).astype(jnp.bfloat16)
+        proj_ref[start : start + rows, :] = jnp.dot(
+            normed, w_ref[...], preferred_element_type=jnp.float32
+        ).astype(jnp.bfloat16)
+    wide = hr * HEAD
+    hq = proj_ref[:, 0:wide].astype(jnp.float32)
+    hf = proj_ref[:, wide : 2 * wide].astype(jnp.float32)
+    hb = proj_ref[:, 2 * wide : 3 * wide].astype(jnp.float32)
+    hv = proj_ref[:, 3 * wide : 4 * wide]
+    queries = hq * jax.nn.sigmoid(hq)
+    taken_f = gap_ref[0:1, :] * jax.nn.sigmoid(-hf)
+    taken_b = gap_ref[1:2, :] * jax.nn.sigmoid(-hb)
+    kept_b = jnp.log1p(-taken_b)
+    kept = jnp.concatenate([jnp.log1p(-taken_f), kept_b], axis=1)
+    row = lax.broadcasted_iota(jnp.int32, (length, length), 0)
+    col = lax.broadcasted_iota(jnp.int32, (length, length), 1)
+    lower = row >= col
+    upper = row <= col
+    ones = jnp.where(lower, 1.0, 0.0).astype(jnp.bfloat16)
+    cumulative = jnp.zeros_like(kept)
+    rest = kept
+    for _ in range(3):
+        part = rest.astype(jnp.bfloat16)
+        rest = rest - part.astype(jnp.float32)
+        cumulative = cumulative + jnp.dot(ones, part, preferred_element_type=jnp.float32)
+    before = cumulative[:, wide:] - kept_b
+    after = cumulative[:, :wide]
+    after = after - 0.5 * after[length - 1 : length, :]
+    before = before - 0.5 * before[length - 1 : length, :]
+    qf = (queries * jnp.exp(after)).astype(jnp.bfloat16)
+    kf = (taken_f * jnp.exp(-after)).astype(jnp.bfloat16)
+    qb = (queries * jnp.exp(-before)).astype(jnp.bfloat16)
+    kb = (taken_b * jnp.exp(before)).astype(jnp.bfloat16)
+    across = (((1,), (1,)), ((), ()))
+    for h in range(hr):
+        span = slice(h * HEAD, (h + 1) * HEAD)
+        fwd = lax.dot_general(qf[:, span], kf[:, span], across, preferred_element_type=jnp.float32)
+        bwd = lax.dot_general(qb[:, span], kb[:, span], across, preferred_element_type=jnp.float32)
+        scores = jnp.where(lower, fwd, 0.0) + jnp.where(upper, bwd, 0.0)
+        out = jnp.dot(scores.astype(jnp.bfloat16), hv[:, span], preferred_element_type=jnp.float32)
+        scale = lax.rsqrt(jnp.mean(out * out, axis=-1, keepdims=True) + epsilon)
+        o_ref[:, span] = (out * scale * hgain_ref[...]).astype(jnp.bfloat16)
+    q_at = 4 * wide
+    k_at = q_at + ha * 2 * DQK
+    v_at = k_at + ha * 2 * DQK
+    for h in range(ha):
+        value = proj_ref[:, v_at + h * DFV : v_at + (h + 1) * DFV]
+        maps = []
+        for m in range(2):
+            offset = (h * 2 + m) * DQK
+            query = proj_ref[:, q_at + offset : q_at + offset + DQK]
+            key = proj_ref[:, k_at + offset : k_at + offset + DQK]
+            scores = lax.dot_general(
+                query, key, across, preferred_element_type=jnp.float32
+            ) * (DQK ** (-0.5))
+            shifted = jnp.exp(scores - jnp.max(scores, axis=-1, keepdims=True))
+            total = jnp.sum(shifted, axis=-1, keepdims=True)
+            accum = jnp.dot(shifted.astype(jnp.bfloat16), value, preferred_element_type=jnp.float32)
+            maps.append(accum / total)
+        weighted = maps[0] - lam_ref[h] * maps[1]
+        scale = lax.rsqrt(jnp.mean(weighted * weighted, axis=-1, keepdims=True) + epsilon)
+        o_ref[:, wide + h * DFV : wide + (h + 1) * DFV] = (
+            weighted * scale * dgain_ref[...] * df_factor
+        ).astype(jnp.bfloat16)
+
+
+def output_kernel(
+    n_sp, n_tp, wide, o_ref, wh_ref, wd_ref, gain_ref, out_ref, og, pbuf, rbuf, s1, r1, s2, r2
+):
+    sp, tp = lax.axis_index("sp"), lax.axis_index("tp")
+    sp_peers = [lax.rem(sp + d, n_sp) for d in range(1, n_sp)]
+    tp_peers = [lax.rem(tp + d, n_tp) for d in range(1, n_tp)]
+    greet([{"sp": p} for p in sp_peers] + [{"tp": p} for p in tp_peers])
+    copies = []
+    for d, peer in enumerate(sp_peers):
+        copy = pltpu.make_async_remote_copy(
+            src_ref=o_ref.at[peer],
+            dst_ref=og.at[sp],
+            send_sem=s1.at[d],
+            recv_sem=r1.at[d],
+            device_id={"sp": peer},
+            device_id_type=MESH,
+        )
+        copy.start()
+        copies.append(copy)
+    og[sp] = o_ref[sp]
+    for copy in copies:
+        copy.wait()
+    hg = jnp.concatenate([og[s, :, :wide] for s in range(n_sp)], axis=1)
+    df = jnp.concatenate([og[s, :, wide:] for s in range(n_sp)], axis=1)
+    partial = jnp.dot(hg, wh_ref[...], preferred_element_type=jnp.float32) + jnp.dot(
+        df, wd_ref[...], preferred_element_type=jnp.float32
+    )
+    pbuf[...] = partial.astype(jnp.bfloat16).reshape(pbuf.shape)
+    copies = []
+    for d, peer in enumerate(tp_peers):
+        copy = pltpu.make_async_remote_copy(
+            src_ref=pbuf.at[peer],
+            dst_ref=rbuf.at[d],
+            send_sem=s2.at[d],
+            recv_sem=r2.at[d],
+            device_id={"tp": peer},
+            device_id_type=MESH,
+        )
+        copy.start()
+        copies.append(copy)
+    mixture = pbuf[tp].astype(jnp.float32)
+    for d, copy in enumerate(copies):
+        copy.wait()
+        mixture = mixture + rbuf[d].astype(jnp.float32)
+    scale = lax.rsqrt(jnp.mean(mixture * mixture, axis=-1, keepdims=True) + epsilon)
+    out_ref[...] = (mixture * scale * gain_ref[...]).astype(jnp.bfloat16)
+
+
+def headwise_shards(
+    n_sp,
+    n_fs,
+    n_tp,
+    inputs,
+    norm_gain,
+    hg_query_w,
+    hg_fwd_w,
+    hg_bwd_w,
+    hg_value_w,
+    floor_gap,
+    hg_norm_gain,
+    df_query_w,
+    df_key_w,
+    df_value_w,
+    diff_lambda,
+    df_norm_gain,
+    out_hg_w,
+    out_df_w,
+    post_gain,
+):
+    x = inputs[0]
+    tokens, depth = x.shape
+    length = tokens * n_sp
+    k_rows = hg_query_w.shape[0]
+    hr = hg_query_w.shape[1] // HEAD // n_sp
+    ha = df_value_w.shape[1] // DFV // n_sp
+    wide = hr * HEAD
+    out_wide = wide + ha * DFV
+    pieces = [hg_query_w, hg_fwd_w, hg_bwd_w, hg_value_w, df_query_w, df_key_w, df_value_w]
+    packed = jnp.concatenate(
+        [w.reshape(k_rows, n_sp, w.shape[1] // n_sp) for w in pieces], axis=2
+    ).transpose(1, 0, 2)
+    columns = packed.shape[2]
+    dma = pltpu.SemaphoreType.DMA
+    weights, rows = pl.pallas_call(
+        functools.partial(gather_kernel, n_sp, n_fs),
+        out_shape=(
+            jax.ShapeDtypeStruct((n_sp, n_fs, k_rows, columns), jnp.bfloat16),
+            jax.ShapeDtypeStruct((n_sp, tokens, depth), jnp.bfloat16),
+        ),
+        in_specs=[VMEM_SPEC, VMEM_SPEC],
+        out_specs=(VMEM_SPEC, VMEM_SPEC),
+        scratch_shapes=[
+            dma((2,)),
+            dma((n_sp - 1,)),
+            dma((n_sp - 1,)),
+            dma((n_sp - 1,)),
+            dma((n_sp - 1,)),
+            dma((n_sp, n_fs - 1)),
+            dma((n_sp, n_fs - 1)),
+        ],
+        compiler_params=pltpu.CompilerParams(collective_id=0, has_side_effects=True),
+        name="gather",
+    )(packed, x)
+    position = lax.axis_index("sp")
+    gap = lax.dynamic_slice_in_dim(floor_gap, position * wide, wide, axis=1)
+    lam = lax.dynamic_slice_in_dim(diff_lambda, position * ha, ha, axis=0)
+    mixed_heads = pl.pallas_call(
+        functools.partial(mixer_kernel, hr, ha),
+        out_shape=jax.ShapeDtypeStruct((length, out_wide), jnp.bfloat16),
+        in_specs=[VMEM_SPEC] * 5 + [pl.BlockSpec(memory_space=pltpu.SMEM), VMEM_SPEC],
+        out_specs=VMEM_SPEC,
+        scratch_shapes=[pltpu.VMEM((length, columns), jnp.bfloat16)],
+        name="mixer",
+    )(
+        rows.reshape(length, depth),
+        weights.reshape(n_sp * n_fs * k_rows, columns),
+        norm_gain[None],
+        gap,
+        hg_norm_gain[None],
+        lam,
+        df_norm_gain[None],
+    )
+    own_rows = tokens // n_tp
+    out = pl.pallas_call(
+        functools.partial(output_kernel, n_sp, n_tp, wide),
+        out_shape=jax.ShapeDtypeStruct((own_rows, depth), jnp.bfloat16),
+        in_specs=[VMEM_SPEC] * 4,
+        out_specs=VMEM_SPEC,
+        scratch_shapes=[
+            pltpu.VMEM((n_sp, tokens, out_wide), jnp.bfloat16),
+            pltpu.VMEM((n_tp, own_rows, depth), jnp.bfloat16),
+            pltpu.VMEM((max(n_tp - 1, 1), own_rows, depth), jnp.bfloat16),
+            dma((n_sp - 1,)),
+            dma((n_sp - 1,)),
+            dma((max(n_tp - 1, 1),)),
+            dma((max(n_tp - 1, 1),)),
+        ],
+        compiler_params=pltpu.CompilerParams(collective_id=1, has_side_effects=True),
+        name="output",
+    )(mixed_heads.reshape(n_sp, tokens, out_wide), out_hg_w, out_df_w, post_gain[None])
+    return out[None]
+
+
+def shards(n_sp, n_fs, n_tp, *arrays):
+    inputs, hg_query_w, df_value_w = arrays[0], arrays[2], arrays[10]
+    heads_hg = hg_query_w.shape[1] // HEAD
+    heads_df = df_value_w.shape[1] // DFV
+    length = inputs.shape[1] * n_sp
+    if heads_hg % n_sp == 0 and heads_df % n_sp == 0 and length * STEEPEST < 60.0:
+        return headwise_shards(n_sp, n_fs, n_tp, *arrays)
+    return spread_shards(*arrays)
+
+
 def solution(mesh):
+    sizes = [mesh.shape[name] for name in ("sp", "fs", "tp")]
     in_specs = (
         P("fs", "sp", None),
         P(),
@@ -247,4 +538,4 @@
         P(),
     )
     out_specs = P("fs", ("sp", "tp"), None)
-    return jax.shard_map(shards, mesh=mesh, in_specs=in_specs, out_specs=out_specs, check_vma=False)
+    return jax.shard_map(functools.partial(shards, *sizes), mesh=mesh, in_specs=in_specs, out_specs=out_specs, check_vma=False)

time: 681 us -> 103 us (0.15)
  waiting for transfers between devices: 342 us -> 0 us
  matrix products: 161 us -> 0 us
  Pallas kernels: 0 us -> 93.4 us
  blocking collectives: 64.8 us -> 0 us
  other arithmetic: 57.5 us -> 0 us
  local copies, waits for them, and re-layouts: 38.5 us -> 9.5 us
  between operations: 13.9 us -> 0.16 us
    all_gather x7 -> x0, waiting for transfers between devices: 331 us -> none  [the longest x1 58.4 us: shards(): lax.all_gather(hg_query_w, ('sp', 'fs'), axis=0, tiled=True)]
    dot_general x29 -> x0, matrix products: 161 us -> none  [the longest x4 120 us: advance(): jnp.einsum('hik,hijk->hij', query_block, decays * key_block[:, None, :, :...]
    pallas_call x0 -> x3, Pallas kernels: none -> 93.4 us  [the longest x1 62.6 us: headwise_shards(): pl.pallas_call(functools.partial(gather_kernel, n_sp, n_fs), out_shape=(j...]
    all_gather x4 -> x0, blocking collectives: 64.8 us -> none  [the longest x1 21.4 us: shards(): lax.all_gather(jnp.stack([fwd_state, bwd_state])[None].astype(jnp.bfloat1...]
    another operation x12 -> x0, other arithmetic: 29.4 us -> none  [the longest x2 24.5 us: summarize(): cumulative_log = jnp.cumsum(series[3], axis=1)]
    mul x7 -> x0, other arithmetic: 10.3 us -> none  [the longest x4 7.4 us: advance(): key_block * jnp.exp(final_log_decay - cumulative_log)]
    select_n x8 -> x0, other arithmetic: 9.25 us -> none  [the longest x4 4.66 us: backward_step(): return jnp.where(member > position, joined, running)]
    reshape x7, local copies, waits for them, and re-layouts: 9.05 us -> 0.96 us  [headwise_shards(): w.reshape(k_rows, n_sp, w.shape[1] // n_sp)]
  transfers between devices with their start and end apart: 8 -> 0, of which waited for: 8 -> 0; matrix products, arithmetic and copies ran while one was open for 8% -> 0% of each run, Pallas kernels for 0% -> 0%
where the time goes in v1:
time: 103 us
  Pallas kernels  93.4 us (91%)
  local copies, waits for them, and re-layouts  9.5 us (9%)
    pallas_call x1, Pallas kernels, headwise_shards(): pl.pallas_call(functools.partial(gather_kernel, n_sp, n_fs), out_shape=(j...  62.6 us
    pallas_call x1, Pallas kernels, headwise_shards(): pl.pallas_call(functools.partial(output_kernel, n_sp, n_tp, wide), out_sh...  21.4 us
    pallas_call x1, Pallas kernels, headwise_shards(): pl.pallas_call(functools.partial(mixer_kernel, hr, ha), out_shape=jax.Sha...  9.39 us
    unnamed x18, local copies, waits for them, and re-layouts  6.18 us

profile of v1, /device:TPU:0, one launch (start us, length us, event | category | flops | bytes accessed | tf_op | source)
XLA Modules:
  0.0 103.0 jit_solution(10243844441656106855)
XLA Ops:
  0.0 0.0 copy-start
  0.0 0.0 copy-start.1
  0.0 0.0 copy-start.2
  0.0 0.0 copy-start.3
  0.0 1.1 %copy.17 = bf16[128,512]{0,1:T(8,128)(2,1)S(1)} copy(bf16[128,512]{1,0:T(8,128)(2,1)} %param.18) | data formatting | bytes 262144 | tf_op args[2]
  1.1 0.1 copy.24
  1.2 1.0 copy.18
  2.3 0.1 copy.25
  2.4 1.0 copy.19
  3.4 0.1 copy.26
  3.6 1.0 copy.20
  4.6 0.0 copy-start.4
  4.6 0.1 copy.27
  4.8 0.0 copy-done.1
  4.8 0.1 copy.21
  4.9 0.1 copy.28
  5.0 0.0 copy-done.2
  5.1 0.1 copy.22
  5.2 0.1 copy.29
  5.3 0.0 copy-done.3
  5.3 0.1 copy.23
  5.4 0.1 copy.30
  5.6 1.1 %concatenate.3 = bf16[128,4,704]{2,0,1:T(8,128)(2,1)} concatenate(bf16[128,4,128]{2,0,1:T(8,128)(2,1)S(1)} %copy.24, bf16[128,4,128]{2,0,1:T(8,128)(2,1)S(1)} %copy.25, bf16[128,4,128]{2,0,1:T(8,128)(2,1)S(1)} %copy.26, bf16[128,4,128]{2,0,1:T(8,128)(2,1)S(1)} %copy.27, bf16[128,4,64]{2,0,1:T(8,128)(2,1)S(1)} %copy.28, bf16[128,4,64]{2,0,1:T(8,128)(2,1)S(1)} %copy.29, ...), dimensions={2} | concatenate | bytes 1441792 | tf_op jit(solution)/shard_map/concatenate | solution.py:445
  6.7 62.6 %gather.1 = (bf16[4,4,128,704]{3,2,1,0:T(8,128)(2,1)}, bf16[4,128,2048]{2,1,0:T(8,128)(2,1)}) custom-call(bf16[4,128,704]{2,1,0:T(8,128)(2,1)} %bitcast.17, bf16[128,2048]{1,0:T(8,128)(2,1)} %bitcast.22), custom_call_target="tpu_custom_call" | custom-call | tf_op jit(solution)/shard_map/gather/pallas_call | solution.py:450
  69.3 0.0 copy-done
  69.3 0.6 constant_dynamic-slice_fusion.gap_ref
  69.9 0.0 copy-done.4
  69.9 0.7 dynamic_slice.7.lam_ref
  70.6 9.4 %mixer.1 = bf16[512,192]{1,0:T(8,128)(2,1)} custom-call(bf16[512,2048]{1,0:T(8,128)(2,1)} %bitcast.19, bf16[2048,704]{1,0:T(8,128)(2,1)} %bitcast.18, f32[1,2048]{1,0:T(1,128)} %bitcast.30, f32[2,128]{1,0:T(2,128)} %constant_dynamic-slice_fusion.gap_ref, f32[1,64]{1,0:T(1,128)} %bitcast.32, f32[1]{0:T(128)} %dynamic_slice.7.lam_ref, f32[1,64]{1,0:T(1,128)} %bitcast.33), custom_call_target="tpu_custom_call" | custom-call | tf_op jit(solution)/shard_map/mixer/pallas_call | solution.py:473
  80.0 21.4 %output.1 = bf16[64,2048]{1,0:T(8,128)(2,1)} custom-call(bf16[4,128,192]{2,1,0:T(8,128)(2,1)} %bitcast.21, bf16[512,2048]{1,0:T(8,128)(2,1)} %wh_ref.1, bf16[256,2048]{1,0:T(8,128)(2,1)} %wd_ref.1, f32[1,2048]{1,0:T(1,128)} %bitcast.31), custom_call_target="tpu_custom_call" | custom-call | tf_op jit(solution)/shard_map/output/pallas_call | solution.py:490
  101.4 1.7 %copy.32 = bf16[1,64,2048]{2,1,0:T(8,128)(2,1)} copy(bf16[1,64,2048]{2,1,0:T(8,128)(2,1)} %bitcast.20) | data formatting | bytes 524288
Async XLA Ops:
  0.0 69.3 %copy-start = (f32[2,512]{1,0:T(2,128)S(1)}, f32[2,512]{1,0:T(2,128)}, u32[]{:S(2)}) copy-start(f32[2,512]{1,0:T(2,128)} %param.22) | copy-start | bytes 12292
  0.0 4.8 %copy-start.1 = (bf16[128,256]{1,0:T(8,128)(2,1)S(1)}, bf16[128,256]{1,0:T(8,128)(2,1)}, u32[]{:S(2)}) copy-start(bf16[128,256]{1,0:T(8,128)(2,1)} %param.24) | copy-start | bytes 196612
  0.0 5.0 %copy-start.2 = (bf16[128,256]{1,0:T(8,128)(2,1)S(1)}, bf16[128,256]{1,0:T(8,128)(2,1)}, u32[]{:S(2)}) copy-start(bf16[128,256]{1,0:T(8,128)(2,1)} %param.25) | copy-start | bytes 196612
  0.0 5.3 %copy-start.3 = (bf16[128,256]{1,0:T(8,128)(2,1)S(1)}, bf16[128,256]{1,0:T(8,128)(2,1)}, u32[]{:S(2)}) copy-start(bf16[128,256]{1,0:T(8,128)(2,1)} %param.26) | copy-start | bytes 196612
  4.6 65.3 %copy-start.4 = (f32[4]{0:T(128)S(1)}, f32[4]{0:T(128)}, u32[]{:S(2)}) copy-start(f32[4]{0:T(128)} %param.27) | copy-start | bytes 52

commit v2 on v0

--- a/solution.py
+++ b/solution.py
@@ -1,6 +1,11 @@
+import functools
+import math
+
 import jax
 import jax.numpy as jnp
 from jax import lax
+from jax.experimental import pallas as pl
+from jax.experimental.pallas import tpu as pltpu
 from jax.sharding import PartitionSpec as P
 
 HEAD = 64
@@ -74,7 +79,7 @@
     return 1
 
 
-def shards(
+def spread_shards(
     inputs,
     norm_gain,
     hg_query_w,
@@ -227,7 +232,342 @@
     return (mixture * rms_scale(mixture) * post_gain).astype(jnp.bfloat16)[None]
 
 
+MESH = pl.DeviceIdType.MESH
+VMEM_SPEC = pl.BlockSpec(memory_space=pltpu.VMEM)
+ANY_SPEC = pl.BlockSpec(memory_space=pl.ANY)
+STEEPEST = -math.log1p(-0.1)
+
+
+LANES = 128
+
+
+def remote(src, dst, send, recv, peer):
+    return pltpu.make_async_remote_copy(
+        src_ref=src, dst_ref=dst, send_sem=send, recv_sem=recv, device_id=peer, device_id_type=MESH
+    )
+
+
+def recurrence(proj_ref, gap, hgain, hr, store):
+    length = proj_ref.shape[0]
+    wide = hr * HEAD
+    hq = proj_ref[:, 0:wide].astype(jnp.bfloat16).astype(jnp.float32)
+    hf = proj_ref[:, wide : 2 * wide].astype(jnp.bfloat16).astype(jnp.float32)
+    hb = proj_ref[:, 2 * wide : 3 * wide].astype(jnp.bfloat16).astype(jnp.float32)
+    hv = proj_ref[:, 3 * wide : 4 * wide].astype(jnp.bfloat16)
+    queries = hq * jax.nn.sigmoid(hq)
+    taken_f = gap[0:1, :] * jax.nn.sigmoid(-hf)
+    taken_b = gap[1:2, :] * jax.nn.sigmoid(-hb)
+    kept_b = jnp.log1p(-taken_b)
+    kept = jnp.concatenate([jnp.log1p(-taken_f), kept_b], axis=1)
+    row = lax.broadcasted_iota(jnp.int32, (length, length), 0)
+    col = lax.broadcasted_iota(jnp.int32, (length, length), 1)
+    lower = row >= col
+    upper = row <= col
+    ones = jnp.where(lower, 1.0, 0.0).astype(jnp.bfloat16)
+    cumulative = jnp.zeros_like(kept)
+    rest = kept
+    for _ in range(3):
+        part = rest.astype(jnp.bfloat16)
+        rest = rest - part.astype(jnp.float32)
+        cumulative = cumulative + jnp.dot(ones, part, preferred_element_type=jnp.float32)
+    before = cumulative[:, wide:] - kept_b
+    after = cumulative[:, :wide]
+    after = after - 0.5 * after[length - 1 : length, :]
+    before = before - 0.5 * before[length - 1 : length, :]
+    qf = (queries * jnp.exp(after)).astype(jnp.bfloat16)
+    kf = (taken_f * jnp.exp(-after)).astype(jnp.bfloat16)
+    qb = (queries * jnp.exp(-before)).astype(jnp.bfloat16)
+    kb = (taken_b * jnp.exp(before)).astype(jnp.bfloat16)
+    across = (((1,), (1,)), ((), ()))
+    for h in range(hr):
+        span = slice(h * HEAD, (h + 1) * HEAD)
+        fwd = lax.dot_general(qf[:, span], kf[:, span], across, preferred_element_type=jnp.float32)
+        bwd = lax.dot_general(qb[:, span], kb[:, span], across, preferred_element_type=jnp.float32)
+        scores = jnp.where(lower, fwd, 0.0) + jnp.where(upper, bwd, 0.0)
+        out = jnp.dot(scores.astype(jnp.bfloat16), hv[:, span], preferred_element_type=jnp.float32)
+        scale = lax.rsqrt(jnp.mean(out * out, axis=-1, keepdims=True) + epsilon)
+        store(span.start, (out * scale * hgain).astype(jnp.bfloat16))
+
+
+def attention(proj_ref, first_lam, lam_ref, dgain, q_at, ha, out_at, store):
+    across = (((1,), (1,)), ((), ()))
+    k_at = q_at + ha * 2 * DQK
+    v_at = k_at + ha * 2 * DQK
+    for h in range(ha):
+        value = proj_ref[:, v_at + h * DFV : v_at + (h + 1) * DFV].astype(jnp.bfloat16)
+        maps = []
+        for m in range(2):
+            offset = (h * 2 + m) * DQK
+            query = proj_ref[:, q_at + offset : q_at + offset + DQK].astype(jnp.bfloat16)
+            key = proj_ref[:, k_at + offset : k_at + offset + DQK].astype(jnp.bfloat16)
+            scores = lax.dot_general(
+                query, key, across, preferred_element_type=jnp.float32
+            ) * (DQK ** (-0.5))
+            shifted = jnp.exp(scores - jnp.max(scores, axis=-1, keepdims=True))
+            total = jnp.sum(shifted, axis=-1, keepdims=True)
+            accum = jnp.dot(shifted.astype(jnp.bfloat16), value, preferred_element_type=jnp.float32)
+            maps.append(accum / total)
+        weighted = maps[0] - lam_ref[first_lam + h] * maps[1]
+        scale = lax.rsqrt(jnp.mean(weighted * weighted, axis=-1, keepdims=True) + epsilon)
+        store(out_at + h * DFV, (weighted * scale * dgain * df_factor).astype(jnp.bfloat16))
+
+
+def block_kernel(
+    n_sp, n_fs, n_tp, hr, ha,
+    x_ref, w0, w1, w2, w3, w4, w5, w6, gain_ref, gap_ref, hgain_ref, lam_ref, dgain_ref,
+    wh_hbm, wd_hbm, post_ref, out_ref,
+    wp, wg, xg, proj, ob, og, pbuf, rbuf, wh, wd,
+    local, s1, r1, sx, rx, sy, ry, s2, r2, s3, r3, s4, r4, s5, r5,
+):
+    sp, fs, tp = lax.axis_index("sp"), lax.axis_index("fs"), lax.axis_index("tp")
+    sp_peers = [lax.rem(sp + d, n_sp) for d in range(1, n_sp)]
+    sp_froms = [lax.rem(sp + n_sp - d, n_sp) for d in range(1, n_sp)]
+    tp_peers = [lax.rem(tp + d, n_tp) for d in range(1, n_tp)]
+    tp_froms = [lax.rem(tp + n_tp - d, n_tp) for d in range(1, n_tp)]
+    paired = n_fs == 4
+    if paired:
+        low, high = lax.rem(fs, 2), fs // 2
+        fs_peers = [high * 2 + 1 - low, (1 - high) * 2 + low]
+        fs_froms = fs_peers
+    else:
+        fs_peers = [lax.rem(fs + e, n_fs) for e in range(1, n_fs)]
+        fs_froms = [lax.rem(fs + n_fs - e, n_fs) for e in range(1, n_fs)]
+    barrier = pltpu.get_barrier_semaphore()
+    peers = (
+        [{"sp": p} for p in sp_peers] + [{"fs": p} for p in fs_peers] + [{"tp": p} for p in tp_peers]
+    )
+    for peer in peers:
+        pl.semaphore_signal(barrier, inc=1, device_id=peer, device_id_type=MESH)
+    load_wh = pltpu.make_async_copy(wh_hbm, wh, local.at[0])
+    load_wd = pltpu.make_async_copy(wd_hbm, wd, local.at[1])
+    tokens, depth = x_ref.shape
+    k_rows = w0.shape[0]
+    wide = hr * HEAD
+    thin = ha * DFV
+    half = k_rows // 2
+    for s in range(n_sp):
+        for b, w in enumerate((w0, w1, w2, w3)):
+            wp[s, b * k_rows : (b + 1) * k_rows, :] = w[:, s * wide : (s + 1) * wide]
+        cut = slice(s * thin, (s + 1) * thin)
+        wp[s, 4 * k_rows : 5 * k_rows, :] = jnp.concatenate([w4[:, cut], w5[:, cut]], axis=1)
+        wp[s, 5 * k_rows :, :] = jnp.concatenate([w6[:half, cut], w6[half:, cut]], axis=1)
+    pl.semaphore_wait(barrier, len(peers))
+
+    started = []
+
+    def send(*args):
+        copy = remote(*args)
+        copy.start()
+        started.append(copy)
+        return copy
+
+    along = [
+        send(wp.at[peer], wg.at[sp, fs], s1.at[d], r1.at[d], {"sp": peer})
+        for d, peer in enumerate(sp_peers)
+    ]
+    across_fs = [
+        [
+            send(wp.at[sp], wg.at[sp, fs], s2.at[0, e], r2.at[0, e], {"fs": peer})
+            for e, peer in enumerate(fs_peers)
+        ]
+    ]
+    share = tokens // n_tp
+    mine = pl.ds(pl.multiple_of(tp * share, share), share)
+    rows_in = [
+        send(x_ref.at[mine, :], xg.at[sp, mine, :], sx.at[d], rx.at[d], {"sp": peer})
+        for d, peer in enumerate(sp_peers)
+    ]
+    load_wh.start()
+    load_wd.start()
+
+    piece_rows = wp.shape[1]
+    cuts = (slice(0, piece_rows // 2), slice(piece_rows // 2, piece_rows))
+    relays = []
+
+    def spread(k):
+        along[k - 1].wait_recv()
+        piece = wg.at[sp_froms[k - 1], fs]
+        across_fs.append(
+            [
+                send(piece, piece, s2.at[k, e], r2.at[k, e], {"fs": peer})
+                for e, peer in enumerate(fs_peers)
+            ]
+        )
+
+    def relay(k):
+        source = sp if k == 0 else sp_froms[k - 1]
+        for e, copy in enumerate(across_fs[k]):
+            copy.wait_recv()
+            if paired:
+                piece = wg.at[source, fs_peers[e], cuts[e], :]
+                relays.append(
+                    (k, send(piece, piece, s5.at[k, e], r5.at[k, e], {"fs": fs_peers[1 - e]}))
+                )
+
+    def normalize(s, rows):
+        x = rows.astype(jnp.float32)
+        scale = lax.rsqrt(jnp.mean(x * x, axis=-1, keepdims=True) + epsilon)
+        xg[s] = (x * scale * gain_ref[...]).astype(jnp.bfloat16)
+
+    wg[sp, fs] = wp[sp]
+    for k in range(1, n_sp):
+        spread(k)
+        relay(k - 1)
+    normalize(sp, x_ref[...])
+    handed = []
+    for d in range(n_sp - 1):
+        rows_in[d].wait_recv()
+        part = xg.at[sp_froms[d], mine, :]
+        handed.append(
+            [
+                send(part, part, sy.at[d, e], ry.at[d, e], {"tp": peer})
+                for e, peer in enumerate(tp_peers)
+            ]
+        )
+    relay(n_sp - 1)
+    for d in range(n_sp - 1):
+        for copy in handed[d]:
+            copy.wait()
+        normalize(sp_froms[d], xg[sp_froms[d]])
+
+    def project(k):
+        source = sp if k == 0 else sp_froms[k - 1]
+        for at, copy in relays:
+            if at == k:
+                copy.wait_recv()
+        blocks = [
+            jnp.concatenate(
+                [wg[source, f, b * k_rows : (b + 1) * k_rows, :] for f in range(n_fs)], axis=0
+            )
+            for b in range(5)
+        ]
+        last = []
+        for f in range(n_fs):
+            tail = wg[source, f, 5 * k_rows :, :]
+            last += [tail[:, :thin], tail[:, thin:]]
+        weights = jnp.concatenate(blocks + [jnp.concatenate(last, axis=0)], axis=1)
+        span = pl.ds(pl.multiple_of(source * (n_fs * k_rows), LANES), n_fs * k_rows)
+        for s in range(n_sp):
+            here = slice(s * tokens, (s + 1) * tokens)
+            added = jnp.dot(xg[s, :, span], weights, preferred_element_type=jnp.float32)
+            if k == 0:
+                proj[here, :] = added
+            else:
+                proj[here, :] += added
+
+    for k in range(n_sp):
+        project(k)
+
+    def store(at, block):
+        width = block.shape[1]
+        for s in range(n_sp):
+            ob[s, :, at : at + width] = block[s * tokens : (s + 1) * tokens]
+
+    gap = gap_ref[:, pl.ds(pl.multiple_of(sp * wide, LANES), wide)]
+    recurrence(proj, gap, hgain_ref[...], hr, store)
+    attention(proj, sp * ha, lam_ref, dgain_ref[...], 4 * wide, ha, wide, store)
+
+    heads = [
+        send(ob.at[peer], og.at[sp], s3.at[d], r3.at[d], {"sp": peer})
+        for d, peer in enumerate(sp_peers)
+    ]
+    og[sp] = ob[sp]
+    load_wh.wait()
+    load_wd.wait()
+    for copy in heads:
+        copy.wait_recv()
+    hg = jnp.concatenate([og[s, :, :wide] for s in range(n_sp)], axis=1)
+    df = jnp.concatenate([og[s, :, wide:] for s in range(n_sp)], axis=1)
+    partial = jnp.dot(hg, wh[...], preferred_element_type=jnp.float32) + jnp.dot(
+        df, wd[...], preferred_element_type=jnp.float32
+    )
+    pbuf[...] = partial.astype(jnp.bfloat16).reshape(pbuf.shape)
+    sums = [
+        send(pbuf.at[peer], rbuf.at[d], s4.at[d], r4.at[d], {"tp": peer})
+        for d, peer in enumerate(tp_peers)
+    ]
+    mixture = pbuf[tp].astype(jnp.float32)
+    for d, copy in enumerate(sums):
+        copy.wait_recv()
+        mixture = mixture + rbuf[d].astype(jnp.float32)
+    scale = lax.rsqrt(jnp.mean(mixture * mixture, axis=-1, keepdims=True) + epsilon)
+    out_ref[...] = (mixture * scale * post_ref[...]).astype(jnp.bfloat16)
+    waited = {id(copy) for group in handed for copy in group}
+    for copy in started:
+        if id(copy) not in waited:
+            copy.wait_send()
+
+
+def headwise_shards(
+    n_sp, n_fs, n_tp,
+    inputs, norm_gain, hg_query_w, hg_fwd_w, hg_bwd_w, hg_value_w, floor_gap, hg_norm_gain,
+    df_query_w, df_key_w, df_value_w, diff_lambda, df_norm_gain, out_hg_w, out_df_w, post_gain,
+):
+    x = inputs[0]
+    tokens, depth = x.shape
+    length = tokens * n_sp
+    k_rows = hg_query_w.shape[0]
+    hr = hg_query_w.shape[1] // HEAD // n_sp
+    ha = df_value_w.shape[1] // DFV // n_sp
+    columns = 4 * hr * HEAD + ha * (4 * DQK + DFV)
+    out_wide = hr * HEAD + ha * DFV
+    own_rows = tokens // n_tp
+    piece = (columns * k_rows // LANES, LANES)
+    low = jnp.bfloat16
+    dma = pltpu.SemaphoreType.DMA
+    step = n_sp - 1
+    turn = n_tp - 1
+    out = pl.pallas_call(
+        functools.partial(block_kernel, n_sp, n_fs, n_tp, hr, ha),
+        out_shape=jax.ShapeDtypeStruct((own_rows, depth), low),
+        in_specs=[VMEM_SPEC] * 11
+        + [pl.BlockSpec(memory_space=pltpu.SMEM), VMEM_SPEC, ANY_SPEC, ANY_SPEC, VMEM_SPEC],
+        out_specs=VMEM_SPEC,
+        scratch_shapes=[
+            pltpu.VMEM((n_sp,) + piece, low),
+            pltpu.VMEM((n_sp, n_fs) + piece, low),
+            pltpu.VMEM((n_sp, tokens, depth), low),
+            pltpu.VMEM((length, columns), jnp.float32),
+            pltpu.VMEM((n_sp, tokens, out_wide), low),
+            pltpu.VMEM((n_sp, tokens, out_wide), low),
+            pltpu.VMEM((n_tp, own_rows, depth), low),
+            pltpu.VMEM((turn, own_rows, depth), low),
+            pltpu.VMEM(out_hg_w.shape, low),
+            pltpu.VMEM(out_df_w.shape, low),
+            dma((2,)),
+            dma((step,)), dma((step,)),
+            dma((step,)), dma((step,)),
+            dma((step, turn)), dma((step, turn)),
+            dma((n_sp, n_fs - 1)), dma((n_sp, n_fs - 1)),
+            dma((step,)), dma((step,)),
+            dma((turn,)), dma((turn,)),
+            dma((n_sp, 2)), dma((n_sp, 2)),
+        ],
+        compiler_params=pltpu.CompilerParams(collective_id=0, has_side_effects=True),
+        name="block",
+    )(
+        x, hg_query_w, hg_fwd_w, hg_bwd_w, hg_value_w, df_query_w, df_key_w, df_value_w,
+        norm_gain[None], floor_gap, hg_norm_gain[None], diff_lambda, df_norm_gain[None],
+        out_hg_w, out_df_w, post_gain[None],
+    )
+    return out[None]
+
+
+def shards(n_sp, n_fs, n_tp, *arrays):
+    inputs, hg_query_w, df_value_w = arrays[0], arrays[2], arrays[10]
+    heads_hg = hg_query_w.shape[1] // HEAD
+    heads_df = df_value_w.shape[1] // DFV
+    length = inputs.shape[1] * n_sp
+    hr, ha = heads_hg // n_sp, heads_df // n_sp
+    whole = heads_hg % n_sp == 0 and heads_df % n_sp == 0 and min(n_sp, n_fs, n_tp) > 1
+    aligned = hr * HEAD == LANES and 4 * ha * DQK == LANES and 2 * ha * DFV == LANES
+    if whole and aligned and length * STEEPEST < 60.0:
+        return headwise_shards(n_sp, n_fs, n_tp, *arrays)
+    return spread_shards(*arrays)
+
+
 def solution(mesh):
+    sizes = [mesh.shape[name] for name in ("sp", "fs", "tp")]
     in_specs = (
         P("fs", "sp", None),
         P(),
@@ -247,4 +587,4 @@
         P(),
     )
     out_specs = P("fs", ("sp", "tp"), None)
-    return jax.shard_map(shards, mesh=mesh, in_specs=in_specs, out_specs=out_specs, check_vma=False)
+    return jax.shard_map(functools.partial(shards, *sizes), mesh=mesh, in_specs=in_specs, out_specs=out_specs, check_vma=False)

time: 681 us -> 64 us (0.09)
  waiting for transfers between devices: 342 us -> 0 us
  matrix products: 161 us -> 0 us
  blocking collectives: 64.8 us -> 0 us
  Pallas kernels: 0 us -> 62 us
  other arithmetic: 57.5 us -> 0 us
  local copies, waits for them, and re-layouts: 38.5 us -> 1.67 us
  between operations: 13.9 us -> 0.01 us
    all_gather x7 -> x0, waiting for transfers between devices: 331 us -> none  [the longest x1 58.4 us: shards(): lax.all_gather(hg_query_w, ('sp', 'fs'), axis=0, tiled=True)]
    dot_general x29 -> x0, matrix products: 161 us -> none  [the longest x4 120 us: advance(): jnp.einsum('hik,hijk->hij', query_block, decays * key_block[:, None, :, :...]
    all_gather x4 -> x0, blocking collectives: 64.8 us -> none  [the longest x1 21.4 us: shards(): lax.all_gather(jnp.stack([fwd_state, bwd_state])[None].astype(jnp.bfloat1...]
    pallas_call x0 -> x1, Pallas kernels: none -> 62 us  [headwise_shards(): pl.pallas_call(functools.partial(block_kernel, n_sp, n_fs, n_tp, hr, ha),...]
    another operation x12 -> x0, other arithmetic: 29.4 us -> none  [the longest x2 24.5 us: summarize(): cumulative_log = jnp.cumsum(series[3], axis=1)]
    mul x7 -> x0, other arithmetic: 10.3 us -> none  [the longest x4 7.4 us: advance(): key_block * jnp.exp(final_log_decay - cumulative_log)]
    select_n x8 -> x0, other arithmetic: 9.25 us -> none  [the longest x4 4.66 us: backward_step(): return jnp.where(member > position, joined, running)]
    reshape x7 -> x0, local copies, waits for them, and re-layouts: 9.05 us -> none  [the longest x5 6.38 us: to_blocks(): tensor.reshape(head_count, blocks, BLOCK, tensor.shape[-1])]
  transfers between devices with their start and end apart: 8 -> 0, of which waited for: 8 -> 0; matrix products, arithmetic and copies ran while one was open for 8% -> 0% of each run, Pallas kernels for 0% -> 0%
where the time goes in v2:
time: 64 us; the launch traced here: 63.7 us
  Pallas kernels  62 us (97%)
  local copies, waits for them, and re-layouts  1.67 us (3%)
    pallas_call x1, Pallas kernels, headwise_shards(): pl.pallas_call(functools.partial(block_kernel, n_sp, n_fs, n_tp, hr, ha),...  62 us
    unnamed x1, local copies, waits for them, and re-layouts  1.67 us

profile of v2, /device:TPU:0, one launch (start us, length us, event | category | flops | bytes accessed | tf_op | source)
XLA Modules:
  0.0 63.7 jit_solution(2456185040174265534)
XLA Ops:
  0.0 62.0 %block.1 = bf16[64,2048]{1,0:T(8,128)(2,1)} custom-call(bf16[128,2048]{1,0:T(8,128)(2,1)} %bitcast.7, bf16[128,512]{1,0:T(8,128)(2,1)} %w0.1, bf16[128,512]{1,0:T(8,128)(2,1)} %w1.1, bf16[128,512]{1,0:T(8,128)(2,1)} %w2.1, bf16[128,512]{1,0:T(8,128)(2,1)} %w3.1, bf16[128,256]{1,0:T(8,128)(2,1)} %w4.1, bf16[128,256]{1,0:T(8,128)(2,1)} %w5.1, ...), custom_call_target="tpu_custom_call" | custom-call | tf_op jit(solution)/shard_map/block/pallas_call | solution.py:520
  62.0 1.7 %copy.18 = bf16[1,64,2048]{2,1,0:T(8,128)(2,1)} copy(bf16[1,64,2048]{2,1,0:T(8,128)(2,1)} %bitcast.6) | data formatting | bytes 524288

commit v3 on v2

--- a/solution.py
+++ b/solution.py
@@ -316,12 +316,17 @@
     n_sp, n_fs, n_tp, hr, ha,
     x_ref, w0, w1, w2, w3, w4, w5, w6, gain_ref, gap_ref, hgain_ref, lam_ref, dgain_ref,
     wh_hbm, wd_hbm, post_ref, out_ref,
-    wp, wg, xg, proj, ob, og, pbuf, rbuf, wh, wd,
+    wp, wg, w_all, xg, proj, ob, og, pbuf, rbuf, wh, wd,
     local, s1, r1, sx, rx, sy, ry, s2, r2, s3, r3, s4, r4, s5, r5,
 ):
     sp, fs, tp = lax.axis_index("sp"), lax.axis_index("fs"), lax.axis_index("tp")
-    sp_peers = [lax.rem(sp + d, n_sp) for d in range(1, n_sp)]
-    sp_froms = [lax.rem(sp + n_sp - d, n_sp) for d in range(1, n_sp)]
+    if n_sp == 4:
+        near, far = lax.rem(sp, 2), sp // 2
+        sp_peers = [far * 2 + 1 - near, (1 - far) * 2 + near, n_sp - 1 - sp]
+        sp_froms = sp_peers
+    else:
+        sp_peers = [lax.rem(sp + d, n_sp) for d in range(1, n_sp)]
+        sp_froms = [lax.rem(sp + n_sp - d, n_sp) for d in range(1, n_sp)]
     tp_peers = [lax.rem(tp + d, n_tp) for d in range(1, n_tp)]
     tp_froms = [lax.rem(tp + n_tp - d, n_tp) for d in range(1, n_tp)]
     paired = n_fs == 4
@@ -373,10 +378,58 @@
     ]
     share = tokens // n_tp
     mine = pl.ds(pl.multiple_of(tp * share, share), share)
-    rows_in = [
-        send(x_ref.at[mine, :], xg.at[sp, mine, :], sx.at[d], rx.at[d], {"sp": peer})
-        for d, peer in enumerate(sp_peers)
-    ]
+
+    has = (sp + 1 < n_sp, sp > 0)
+    toward = (lax.rem(sp + 1, n_sp), lax.rem(sp + n_sp - 1, n_sp))
+
+    def holds(way, hops):
+        return sp >= hops if way == 0 else sp + hops < n_sp
+
+    def origin(way, hops):
+        return lax.rem(sp + n_sp - hops, n_sp) if way == 0 else lax.rem(sp + hops, n_sp)
+
+    def hop(way, hops):
+        source = origin(way, hops)
+        place = xg.at[source, mine, :]
+        src = x_ref.at[mine, :] if hops == 0 else place
+        return remote(src, place, sx.at[way, hops], rx.at[way, hops], {"sp": toward[way]})
+
+    def hand(way, hops, e):
+        part = xg.at[origin(way, hops + 1), mine, :]
+        return remote(part, part, sy.at[way, hops, e], ry.at[way, hops, e], {"tp": tp_peers[e]})
+
+    def push(hops):
+        for way in range(2):
+            @pl.when(holds(way, hops) & has[way])
+            def _():
+                hop(way, hops).start()
+
+    def take(hops):
+        for way in range(2):
+            @pl.when(holds(way, hops + 1))
+            def _():
+                hop(way, hops).wait_recv()
+                if hops + 1 < n_sp - 1:
+                    @pl.when(has[way])
+                    def _():
+                        hop(way, hops + 1).start()
+                for e in range(n_tp - 1):
+                    hand(way, hops, e).start()
+
+    def finish(hops):
+        for way in range(2):
+            @pl.when(holds(way, hops + 1))
+            def _():
+                for e in range(n_tp - 1):
+                    hand(way, hops, e).wait()
+                if hops + 1 < n_sp - 1:
+                    @pl.when(has[way])
+                    def _():
+                        hop(way, hops + 1).wait_send()
+                source = origin(way, hops + 1)
+                normalize(source, xg[source])
+
+    push(0)
     load_wh.start()
     load_wd.start()
 
@@ -409,54 +462,39 @@
         scale = lax.rsqrt(jnp.mean(x * x, axis=-1, keepdims=True) + epsilon)
         xg[s] = (x * scale * gain_ref[...]).astype(jnp.bfloat16)
 
-    wg[sp, fs] = wp[sp]
-    for k in range(1, n_sp):
-        spread(k)
-        relay(k - 1)
-    normalize(sp, x_ref[...])
-    handed = []
-    for d in range(n_sp - 1):
-        rows_in[d].wait_recv()
-        part = xg.at[sp_froms[d], mine, :]
-        handed.append(
-            [
-                send(part, part, sy.at[d, e], ry.at[d, e], {"tp": peer})
-                for e, peer in enumerate(tp_peers)
-            ]
-        )
-    relay(n_sp - 1)
-    for d in range(n_sp - 1):
-        for copy in handed[d]:
-            copy.wait()
-        normalize(sp_froms[d], xg[sp_froms[d]])
-
-    def project(k):
+    def assemble(k):
         source = sp if k == 0 else sp_froms[k - 1]
         for at, copy in relays:
             if at == k:
                 copy.wait_recv()
-        blocks = [
-            jnp.concatenate(
-                [wg[source, f, b * k_rows : (b + 1) * k_rows, :] for f in range(n_fs)], axis=0
-            )
-            for b in range(5)
-        ]
-        last = []
         for f in range(n_fs):
+            first = source * (n_fs * k_rows) + f * k_rows
+            for b in range(5):
+                w_all[pl.ds(pl.multiple_of(first, half), k_rows), b * LANES : (b + 1) * LANES] = wg[
+                    source, f, b * k_rows : (b + 1) * k_rows, :
+                ]
             tail = wg[source, f, 5 * k_rows :, :]
-            last += [tail[:, :thin], tail[:, thin:]]
-        weights = jnp.concatenate(blocks + [jnp.concatenate(last, axis=0)], axis=1)
-        span = pl.ds(pl.multiple_of(source * (n_fs * k_rows), LANES), n_fs * k_rows)
-        for s in range(n_sp):
-            here = slice(s * tokens, (s + 1) * tokens)
-            added = jnp.dot(xg[s, :, span], weights, preferred_element_type=jnp.float32)
-            if k == 0:
-                proj[here, :] = added
-            else:
-                proj[here, :] += added
-
-    for k in range(n_sp):
-        project(k)
+            w_all[pl.ds(pl.multiple_of(first, half), half), 5 * LANES :] = tail[:, :thin]
+            w_all[pl.ds(pl.multiple_of(first + half, half), half), 5 * LANES :] = tail[:, thin:]
+
+    wg[sp, fs] = wp[sp]
+    normalize(sp, x_ref[...])
+    for k in range(1, n_sp):
+        spread(k)
+        relay(k - 1)
+    take(0)
+    assemble(0)
+    relay(n_sp - 1)
+    for hops in range(1, n_sp - 1):
+        assemble(hops)
+        take(hops)
+    finish(0)
+    assemble(n_sp - 1)
+    for hops in range(1, n_sp - 1):
+        finish(hops)
+    proj[...] = jnp.dot(
+        xg[...].reshape(n_sp * tokens, depth), w_all[...], preferred_element_type=jnp.float32
+    )
 
     def store(at, block):
         width = block.shape[1]
@@ -492,10 +530,12 @@
         mixture = mixture + rbuf[d].astype(jnp.float32)
     scale = lax.rsqrt(jnp.mean(mixture * mixture, axis=-1, keepdims=True) + epsilon)
     out_ref[...] = (mixture * scale * post_ref[...]).astype(jnp.bfloat16)
-    waited = {id(copy) for group in handed for copy in group}
     for copy in started:
-        if id(copy) not in waited:
-            copy.wait_send()
+        copy.wait_send()
+    for way in range(2):
+        @pl.when(has[way])
+        def _():
+            hop(way, 0).wait_send()
 
 
 def headwise_shards(
@@ -526,6 +566,7 @@
         scratch_shapes=[
             pltpu.VMEM((n_sp,) + piece, low),
             pltpu.VMEM((n_sp, n_fs) + piece, low),
+            pltpu.VMEM((n_sp * n_fs * k_rows, columns), low),
             pltpu.VMEM((n_sp, tokens, depth), low),
             pltpu.VMEM((length, columns), jnp.float32),
             pltpu.VMEM((n_sp, tokens, out_wide), low),
@@ -536,8 +577,8 @@
             pltpu.VMEM(out_df_w.shape, low),
             dma((2,)),
             dma((step,)), dma((step,)),
-            dma((step,)), dma((step,)),
-            dma((step, turn)), dma((step, turn)),
+            dma((2, step)), dma((2, step)),
+            dma((2, step, turn)), dma((2, step, turn)),
             dma((n_sp, n_fs - 1)), dma((n_sp, n_fs - 1)),
             dma((step,)), dma((step,)),
             dma((turn,)), dma((turn,)),

time: 64 us -> 59.8 us (0.934)
  Pallas kernels: 62 us -> 57.9 us
    pallas_call x1, Pallas kernels: 62 us -> 57.9 us  [headwise_shards(): pl.pallas_call(functools.partial(block_kernel, n_sp, n_fs, n_tp, hr, ha),...]
where the time goes in v3:
time: 59.8 us; the launch traced here: 59.5 us
  Pallas kernels  57.9 us (97%)
  local copies, waits for them, and re-layouts  1.67 us (3%)
    pallas_call x1, Pallas kernels, headwise_shards(): pl.pallas_call(functools.partial(block_kernel, n_sp, n_fs, n_tp, hr, ha),...  57.9 us
    unnamed x1, local copies, waits for them, and re-layouts  1.67 us

profile of v3, /device:TPU:0, one launch (start us, length us, event | category | flops | bytes accessed | tf_op | source)
XLA Modules:
  0.0 59.5 jit_solution(2436382420843401443)
XLA Ops:
  0.0 57.9 %block.1 = bf16[64,2048]{1,0:T(8,128)(2,1)} custom-call(bf16[128,2048]{1,0:T(8,128)(2,1)} %bitcast.7, bf16[128,512]{1,0:T(8,128)(2,1)} %w0.1, bf16[128,512]{1,0:T(8,128)(2,1)} %w1.1, bf16[128,512]{1,0:T(8,128)(2,1)} %w2.1, bf16[128,512]{1,0:T(8,128)(2,1)} %w3.1, bf16[128,256]{1,0:T(8,128)(2,1)} %w4.1, bf16[128,256]{1,0:T(8,128)(2,1)} %w5.1, ...), custom_call_target="tpu_custom_call" | custom-call | tf_op jit(solution)/shard_map/block/pallas_call | solution.py:560
  57.9 1.7 %copy.18 = bf16[1,64,2048]{2,1,0:T(8,128)(2,1)} copy(bf16[1,64,2048]{2,1,0:T(8,128)(2,1)} %bitcast.6) | data formatting | bytes 524288
